TPU v7x, 32 devices: a whole 2x2x4 slice. The times are simulated.
32 devices in a mesh: grp: 2 (over y), sp: 4 (over z), tp: 4 (over x, core).
Axes of the slice: x: 2, y: 2, z: 4, core: 2. Of those that a mesh axis runs over, the one named last changes fastest.
Arguments:
- tokens: bfloat16 [3072, 2048], P(('grp', 'sp'), 'tp'), parts along dimension 0, may hold values from -6 to 6
- norm_gain: float32 [2048], replicated, may hold values from 0.1 to 1.9
- qk_gain: float32 [4, 64], replicated, may hold values from 0.7 to 5.5
- w_query_window: bfloat16 [2048, 1024], P('sp', 'tp'), may hold values from -1 to 1
- w_key_window: bfloat16 [2048, 512], P('sp', 'tp'), may hold values from -1 to 1
- w_value_window: bfloat16 [2048, 512], P('sp', 'tp'), may hold values from -0.125 to 0.125
- sink_logits: float32 [16], P('tp'), may hold values from 0 to 5
- w_query_forget: bfloat16 [2048, 1024], P('sp', 'tp'), may hold values from -1 to 1
- w_key_forget: bfloat16 [2048, 1024], P('sp', 'tp'), may hold values from -1 to 1
- w_value_forget: bfloat16 [2048, 1024], P('sp', 'tp'), may hold values from -0.125 to 0.125
- gate_cum: float32 [3072, 16], P(('grp', 'sp'), 'tp'), parts along dimension 0, as said below
- w_merge: bfloat16 [2048, 2, 2048], P('sp', None, 'tp'), may hold values from -0.125 to 0.125
- w_branch: bfloat16 [2, 1024, 2048], P(None, 'sp', 'tp'), may hold values from -0.8984375 to 0.8984375
Outputs:
- mixed: bfloat16 [3072, 2048], P(('grp', 'sp'), 'tp'), parts along dimension 0
There are 2 independent parts, one for each index of `grp`. A program takes and returns all parts, laid end to end along the dimension named above; an argument that names none is the same for every part. Nothing has to cross between parts.
Inputs may be any that keep to these rules, and one draw needn't show every extreme that they name: `gate_cum`: along positions each head's values never rise.
All inputs are finite; a program needn't handle non-finite values.
Results may differ from a plain program's by a relative error of at most 0.012.
Values may be sent and summed in bfloat16 or wider, within the bound.
A program may use at most 64 MiB of HBM per device.

v0:
```python
import math
import jax
import jax.numpy as jnp
from jax import lax
from jax.sharding import PartitionSpec as P

HEAD = 64
WINDOW = 128
epsilon = 1e-06
big_negative = -1e30


def from_behind(value, axis, by):
    size = lax.axis_size(axis)
    pairs = [(i, i + by) for i in range(size) if 0 <= i + by < size]
    return lax.ppermute(value, axis, pairs)


def head_norm(raw, gain, head_count):
    split = raw.reshape(raw.shape[0], head_count, -1)
    scaled = split * lax.rsqrt(jnp.mean(split * split, axis=-1, keepdims=True) + epsilon) * gain
    return scaled.astype(jnp.bfloat16)


def window_attend(queries, keys_ext, values_ext, sink_rows, first_pos):
    row_count, head_count, head_size = queries.shape
    group_count = keys_ext.shape[1]
    span_rows = WINDOW // 2
    block_count = row_count // span_rows
    query_blocks = queries.reshape(
        block_count, span_rows, group_count, head_count // group_count, head_size
    )
    key_blocks = jnp.concatenate(
        [
            keys_ext[lag_index * span_rows : lag_index * span_rows + row_count].reshape(
                block_count, span_rows, group_count, head_size
            )
            for lag_index in range(3)
        ],
        axis=1,
    )
    value_blocks = jnp.concatenate(
        [
            values_ext[lag_index * span_rows : lag_index * span_rows + row_count].reshape(
                block_count, span_rows, group_count, head_size
            )
            for lag_index in range(3)
        ],
        axis=1,
    )
    scores = jnp.einsum(
        "nqgrd,nkgd->ngrqk", query_blocks, key_blocks, preferred_element_type=jnp.float32
    ) * head_size ** (-0.5)
    distance = WINDOW + jnp.arange(span_rows)[:, None] - jnp.arange(3 * span_rows)[None, :]
    key_pos = (
        first_pos
        - WINDOW
        + jnp.arange(block_count)[:, None] * span_rows
        + jnp.arange(3 * span_rows)[None, :]
    )
    is_valid = ((distance >= 0) & (distance < WINDOW))[None] & (key_pos >= 0)[:, None, :]
    is_valid = is_valid[:, None, None]
    sink_grid = sink_rows.reshape(1, group_count, head_count // group_count, 1)
    row_max = jnp.maximum(jnp.max(jnp.where(is_valid, scores, big_negative), axis=-1), sink_grid)
    weights = jnp.where(is_valid, jnp.exp(scores - row_max[..., None]), 0.0)
    row_total = jnp.sum(weights, axis=-1) + jnp.exp(sink_grid - row_max)
    prob_rows = (weights / row_total[..., None]).astype(jnp.bfloat16)
    mixed_sum = jnp.einsum(
        "ngrqk,nkgd->nqgrd", prob_rows, value_blocks, preferred_element_type=jnp.float32
    )
    return mixed_sum.reshape(row_count, head_count * head_size).astype(jnp.bfloat16)


def forget_groups(groups, keys, values, gates):
    head_count, head_size = (keys.shape[1], keys.shape[2])
    gates_all = lax.all_gather(gates, "sp", axis=0, tiled=True)

    def absorber(queries, query_gate, query_pos):

        def absorb(running, block):
            row_max, row_total, mixed_sum = running
            key_rows, value_rows, key_gate, key_pos = block
            scores = jnp.einsum(
                "qhd,khd->hqk", queries, key_rows, preferred_element_type=jnp.float32
            ) * head_size ** (-0.5)
            scores = scores + query_gate.T[:, :, None] - key_gate.T[:, None, :]
            is_valid = (query_pos[:, None] >= key_pos[None, :])[None]
            new_max = jnp.maximum(
                row_max, jnp.max(jnp.where(is_valid, scores, big_negative), axis=-1)
            )
            weights = jnp.where(is_valid, jnp.exp(scores - new_max[..., None]), 0.0)
            shrink = jnp.exp(row_max - new_max)
            row_total = row_total * shrink + jnp.sum(weights, axis=-1)
            mixed_sum = mixed_sum * shrink.T[:, :, None] + jnp.einsum(
                "hqk,khd->qhd",
                weights.astype(jnp.bfloat16),
                value_rows,
                preferred_element_type=jnp.float32,
            )
            return ((new_max, row_total, mixed_sum), None)

        return absorb

    initial = tuple(
        (
            (
                jnp.full((head_count, group[0].shape[0]), big_negative, jnp.float32),
                jnp.zeros((head_count, group[0].shape[0]), jnp.float32),
                jnp.zeros((group[0].shape[0], head_count, head_size), jnp.float32),
            )
            for group in groups
        )
    )
    first_row = jnp.int32(0)
    key_rows = lax.all_gather(keys, "sp", axis=0, tiled=True)
    value_rows = lax.all_gather(values, "sp", axis=0, tiled=True)
    piece_rows = key_rows.shape[0]
    sub_rows = math.gcd(piece_rows, 2048)
    turns = piece_rows // sub_rows
    key_gate = gates_all
    key_pos = jnp.arange(piece_rows)
    blocks = (
        key_rows.reshape(turns, sub_rows, head_count, head_size),
        value_rows.reshape(turns, sub_rows, head_count, head_size),
        key_gate.reshape(turns, sub_rows, head_count),
        key_pos.reshape(turns, sub_rows),
    )
    updated = []
    for (queries, query_gate, query_pos), state in zip(groups, initial):
        absorb = absorber(queries, query_gate, query_pos)

        def advance(current):
            return lax.scan(absorb, current, blocks)[0]

        def keep(current):
            return current

        updated.append(lax.cond(first_row <= query_pos[-1], advance, keep, state))
    finals = tuple(updated)
    return [
        (mixed_sum / row_total.T[:, :, None])
        .reshape(mixed_sum.shape[0], head_count * head_size)
        .astype(jnp.bfloat16)
        for row_max, row_total, mixed_sum in finals
    ]


def on_device(
    tokens,
    norm_gain,
    qk_gain,
    w_query_window,
    w_key_window,
    w_value_window,
    sink_logits,
    w_query_forget,
    w_key_forget,
    w_value_forget,
    gate_cum,
    w_merge,
    w_branch,
):
    row_count = tokens.shape[0]
    row_offset = lax.axis_index("sp") * row_count
    gathered = lax.all_gather(tokens, "tp", axis=1, tiled=True)
    as_float = gathered.astype(jnp.float32)
    normed = (
        as_float
        * lax.rsqrt(jnp.mean(as_float * as_float, axis=-1, keepdims=True) + epsilon)
        * norm_gain
    ).astype(jnp.bfloat16)
    merge_flat = w_merge.reshape(w_merge.shape[0], -1)
    pieces = (
        lax.all_gather(w_query_window, "sp", axis=0, tiled=True),
        lax.all_gather(w_key_window, "sp", axis=0, tiled=True),
        lax.all_gather(w_value_window, "sp", axis=0, tiled=True),
        lax.all_gather(w_query_forget, "sp", axis=0, tiled=True),
        lax.all_gather(w_key_forget, "sp", axis=0, tiled=True),
        lax.all_gather(w_value_forget, "sp", axis=0, tiled=True),
        lax.all_gather(merge_flat, "sp", axis=0, tiled=True),
    )
    projected = tuple(
        (jnp.dot(normed, weight_rows, preferred_element_type=jnp.float32) for weight_rows in pieces)
    )
    query_heads = w_query_window.shape[1] // HEAD
    group_heads = w_key_window.shape[1] // HEAD
    window_query = head_norm(projected[0], qk_gain[0], query_heads)
    window_key = head_norm(projected[1], qk_gain[1], group_heads)
    window_value = projected[2].astype(jnp.bfloat16).reshape(row_count, group_heads, HEAD)
    prev_key, prev_value = from_behind(
        (window_key[row_count - WINDOW :], window_value[row_count - WINDOW :]), "sp", 1
    )
    window_out = window_attend(
        window_query,
        jnp.concatenate([prev_key, window_key], axis=0),
        jnp.concatenate([prev_value, window_value], axis=0),
        sink_logits,
        row_offset,
    )
    forget_query = head_norm(projected[3], qk_gain[2], query_heads)
    forget_key = head_norm(projected[4], qk_gain[3], query_heads)
    forget_value = projected[5].astype(jnp.bfloat16).reshape(row_count, query_heads, HEAD)
    own_pos = row_offset + jnp.arange(row_count)
    forget_out = forget_groups(
        [(forget_query, gate_cum, own_pos)], forget_key, forget_value, gate_cum
    )[0]
    channel_count = w_merge.shape[2]
    merge_gate = jax.nn.sigmoid(projected[6]).reshape(row_count, 2, channel_count)
    branch_full = lax.all_gather(w_branch, "sp", axis=1, tiled=True)
    head_stack = jnp.stack([window_out, forget_out], axis=1)
    weight_rows = branch_full
    projection = jnp.einsum(
        "uxa,xag->uxg",
        lax.all_gather(head_stack, "tp", axis=2, tiled=True),
        weight_rows,
        preferred_element_type=jnp.float32,
    )
    return (merge_gate[:, 0] * projection[:, 0] + merge_gate[:, 1] * projection[:, 1]).astype(
        jnp.bfloat16
    )


def solution(mesh):
    return jax.shard_map(
        on_device,
        mesh=mesh,
        in_specs=(
            P(("grp", "sp"), "tp"),
            P(),
            P(),
            P("sp", "tp"),
            P("sp", "tp"),
            P("sp", "tp"),
            P("tp"),
            P("sp", "tp"),
            P("sp", "tp"),
            P("sp", "tp"),
            P(("grp", "sp"), "tp"),
            P("sp", None, "tp"),
            P(None, "sp", "tp"),
        ),
        out_specs=P(("grp", "sp"), "tp"),
        check_vma=False,
    )
```

profile of v0, /device:TPU:0, one launch (start us, length us, event | category | flops | bytes accessed | tf_op | source)
XLA Modules:
  0.0 339.6 jit_solution(14842164746860835694)
XLA Ops:
  6.6 0.7 all-gather.9.cloned.1.call-update
  7.3 0.7 all-gather.15.cloned.1.call-update
  8.1 0.7 all-gather.17.cloned.1.call-update
  11.2 1.3 slice.58
  13.7 16.6 %all_gather.48 = f32[1536,4]{0,1:T(4,128)} all-gather(f32[384,4]{0,1:T(4,128)} %param.27), channel_id=1, replica_groups=mesh['grp'=2,'sp'=4,'tp'=4] {'sp'}, dimensions={0}, use_global_device_ids=true | all-gather | bytes 30720 | tf_op jit(solution)/shard_map/all_gather | solution.py:76
  30.5 19.0 %all_gather.42 = bf16[2048,128]{1,0:T(8,128)(2,1)} all-gather(bf16[512,128]{1,0:T(8,128)(2,1)S(1)} %copy-done.8), channel_id=1, replica_groups=mesh['grp'=2,'sp'=4,'tp'=4] {'sp'}, dimensions={0}, use_global_device_ids=true | all-gather | bytes 655360 | tf_op jit(solution)/shard_map/all_gather | solution.py:175
  49.5 0.7 max.20
  50.2 21.1 %all_gather.41 = bf16[2048,128]{1,0:T(8,128)(2,1)} all-gather(bf16[512,128]{1,0:T(8,128)(2,1)S(1)} %copy-done.9), channel_id=1, replica_groups=mesh['grp'=2,'sp'=4,'tp'=4] {'sp'}, dimensions={0}, use_global_device_ids=true | all-gather | bytes 655360 | tf_op jit(solution)/shard_map/all_gather | solution.py:176
  71.2 0.7 broadcast_and_fusion
  71.9 1.9 fusion.25
  74.3 2.5 multiply_reduce_fusion.1
  77.0 25.4 %all_gather.45 = bf16[1536,4,64]{0,2,1:T(8,128)(2,1)S(1)} all-gather(bf16[384,4,64]{0,2,1:T(8,128)(2,1)S(1)} %multiply_convert_fusion.2), channel_id=1, replica_groups=mesh['grp'=2,'sp'=4,'tp'=4] {'sp'}, dimensions={0}, use_global_device_ids=true | all-gather | bytes 983040 | tf_op jit(solution)/shard_map/all_gather | solution.py:115
  102.5 5.3 %all-gather.17.cloned.1.call-done = bf16[2048,256]{1,0:T(8,128)(2,1)} async-done(((bf16[512,256]{1,0:T(8,128)(2,1)}), bf16[2048,256]{1,0:T(8,128)(2,1)}) %all-gather.17.cloned.1.call-update) | async-done | bytes 1048592 | tf_op jit(solution)/shard_map/all_gather | solution.py:179
  107.7 2.0 convolution_convert_fusion.1
  109.7 25.2 %all_gather.47 = bf16[1536,4,64]{0,2,1:T(8,128)(2,1)S(1)} all-gather(bf16[384,4,64]{0,2,1:T(8,128)(2,1)S(1)} %bitcast.165), channel_id=1, replica_groups=mesh['grp'=2,'sp'=4,'tp'=4] {'sp'}, dimensions={0}, use_global_device_ids=true | all-gather | bytes 983040 | tf_op jit(solution)/shard_map/all_gather | solution.py:116
  134.9 8.7 %all-gather.19.cloned.1.call-done = bf16[2048,256]{1,0:T(8,128)(2,1)} async-done(((bf16[512,256]{1,0:T(8,128)(2,1)}), bf16[2048,256]{1,0:T(8,128)(2,1)}) %all-gather.19.cloned.1.call-update) | async-done | bytes 1048592 | tf_op jit(solution)/shard_map/all_gather | solution.py:177
  143.7 2.1 multiply_reduce_fusion
  145.7 1.2 multiply_reduce_fusion.2
  147.0 1.2 convolution_convert_fusion.2
  148.2 0.8 multiply_convert_fusion.1
  149.0 35.5 %conditional.1 = (f32[4,384]{1,0:T(4,128)}, f32[384,4,64]{0,2,1:T(8,128)}) conditional(s32[]{:T(128)} %bitcast.13, () %tuple.20, (bf16[1536,4,64]{0,2,1:T(8,128)(2,1)S(1)}, bf16[1536,4,64]{0,2,1:T(8,128)(2,1)S(1)}, f32[1536,4]{0,1:T(4,128)}, s32[3,512]{1,0:T(4,128)S(1)}, s32[3,512]{1,0:T(4,128)S(1)}, /*index=5*/s32[384]{0:T(512)}, ...), branch_computations={%region_7.8_spmd, %region_8.13_spmd} | conditional | flops 215199744 | bytes 15060769 | solution.py:138
  149.6 1.4 copy_bitcast_fusion
  151.0 33.5 %while.18 = (s32[]{:T(128)}, f32[4,384]{1,0:T(4,128)S(1)}, f32[4,384]{1,0:T(4,128)}, f32[384,4,64]{0,2,1:T(8,128)}, s32[384]{0:T(512)}, /*index=5*/s32[3,512]{1,...) while((s32[]{:T(128)}, f32[4,384]{1,0:T(4,128)S(1)}, ...), condition=%wide.region_12.12_spmd.clone, body=%wide.region_9.11_spmd.clone.sunk | while | flops 215196672 | bytes 11896481 | solution.py:133
  151.0 0.7 dynamic-slice_bitcast_fusion.2
  151.7 0.7 constant_dynamic-slice_fusion.2
  152.4 0.9 broadcast_compare_fusion.2
  153.2 2.7 fusion.85
  155.9 0.7 fusion.86
  156.6 1.6 fusion.87
  158.2 0.6 fusion.88
  158.8 2.7 fusion.89
  161.6 0.7 dynamic-slice_bitcast_fusion.2
  162.3 0.7 constant_dynamic-slice_fusion.2
  163.0 0.9 broadcast_compare_fusion.2
  163.8 2.7 fusion.85
  166.5 0.7 fusion.86
  167.2 1.6 fusion.87
  168.8 1.3 fusion.88
  170.1 2.9 fusion.89
  173.0 0.7 dynamic-slice_bitcast_fusion.2
  173.7 0.7 constant_dynamic-slice_fusion.2
  174.4 0.9 broadcast_compare_fusion.2
  175.3 2.7 fusion.85
  178.0 0.7 fusion.86
  178.7 1.6 fusion.87
  180.3 1.3 fusion.88
  181.6 2.9 fusion.89
  184.5 1.0 divide_convert_fusion.2
  185.5 2.5 bitcast_reduce_fusion
  189.8 2.8 collective-permute-start.1
  192.6 3.3 collective-permute-start
  195.9 1.0 multiply_convert_fusion
  199.2 0.6 fusion.31
  200.0 1.0 fusion.32
  201.6 0.8 pad_maximum_fusion
  202.5 1.3 copy.55
  203.8 14.9 %all-gather.23.cloned.1.call-done = bf16[2,1024,512]{2,1,0:T(8,128)(2,1)} async-done(((bf16[2,256,512]{2,1,0:T(8,128)(2,1)}), bf16[2,1024,512]{2,1,0:T(8,128)(2,1)}) %all-gather.23.cloned.1.call-update) | async-done | bytes 2097168 | tf_op jit(solution)/shard_map/all_gather | solution.py:209
  218.6 21.5 %all-gather.21.cloned.1.call-done = bf16[384,2,1024]{2,0,1:T(8,128)(2,1)} async-done(((bf16[384,2,256]{2,0,1:T(8,128)(2,1)}), bf16[384,2,1024]{2,0,1:T(8,128)(2,1)}) %all-gather.21.cloned.1.call-update) | async-done | bytes 1572880 | tf_op jit(solution)/shard_map/all_gather | solution.py:214
  240.2 3.0 convolution_bitcast_fusion
  243.2 79.3 %all-gather.11.cloned.1.call-done = bf16[2048,1024]{1,0:T(8,128)(2,1)} async-done(((bf16[512,1024]{1,0:T(8,128)(2,1)}), bf16[2048,1024]{1,0:T(8,128)(2,1)}) %all-gather.11.cloned.1.call-update) | async-done | bytes 4194320 | tf_op jit(solution)/shard_map/all_gather | solution.py:180
  322.5 5.3 %add_divide_fusion = f32[384,1024]{1,0:T(8,128)} fusion(bf16[384,2048]{1,0:T(8,128)(2,1)S(1)} %copy-done.1, bf16[2048,1024]{1,0:T(8,128)(2,1)} %all-gather.11.cloned.1.call-done), kind=kOutput, calls=%fused_computation.44 | convolution fusion | flops 1611792384 | bytes 7340032 | tf_op jit(solution)/shard_map/dot_general | solution.py:183
  327.8 2.6 reshape.258
  330.5 1.2 fusion.56
  331.7 1.0 fusion.36
  (103 shorter events, 9.1 us)
Async XLA Ops:
  6.5 6.6 %copy-start.15 = (f32[4,64]{1,0:T(4,128)S(1)}, f32[4,64]{1,0:T(4,128)}, u32[]{:S(2)}) copy-start(f32[4,64]{1,0:T(4,128)} %param.19) | copy-start | bytes 3076
  6.5 24.0 %copy-start.8 = (bf16[512,128]{1,0:T(8,128)(2,1)S(1)}, bf16[512,128]{1,0:T(8,128)(2,1)}, u32[]{:S(2)}) copy-start(bf16[512,128]{1,0:T(8,128)(2,1)} %param.21) | copy-start | bytes 393220
  6.5 42.9 %copy-start.16 = (f32[4]{0:T(128)S(1)}, f32[4]{0:T(128)}, u32[]{:S(2)}) copy-start(f32[4]{0:T(128)} %param.23) | copy-start | bytes 52
  6.5 43.6 %copy-start.9 = (bf16[512,128]{1,0:T(8,128)(2,1)S(1)}, bf16[512,128]{1,0:T(8,128)(2,1)}, u32[]{:S(2)}) copy-start(bf16[512,128]{1,0:T(8,128)(2,1)} %param.22) | copy-start | bytes 393220
  6.5 65.4 %all-gather.9.cloned.1.call-start = ((), (), s32[]{:S(2)}) async-start(), calls=%async_computation | async-start | bytes 1966080 | tf_op jit(solution)/shard_map/all_gather | solution.py:165
  7.3 67.1 %all-gather.15.cloned.1.call-start = ((), (), s32[]{:S(2)}) async-start(), calls=%async_computation.3 | async-start | bytes 1310720 | tf_op jit(solution)/shard_map/all_gather | solution.py:178
  8.0 99.7 %all-gather.17.cloned.1.call-start = ((), (), s32[]{:S(2)}) async-start(), calls=%async_computation.4 | async-start | bytes 1310720 | tf_op jit(solution)/shard_map/all_gather | solution.py:179
  8.8 134.9 %all-gather.19.cloned.1.call-start = ((), (), s32[]{:S(2)}) async-start(), calls=%async_computation.5 | async-start | bytes 1310720 | tf_op jit(solution)/shard_map/all_gather | solution.py:177
  9.3 176.2 %all-gather.13.cloned.1.call-start = ((), (), s32[]{:S(2)}) async-start(), calls=%async_computation.2 | async-start | bytes 1310720 | tf_op jit(solution)/shard_map/all_gather | solution.py:174
  9.9 208.7 %all-gather.23.cloned.1.call-start = ((), (), s32[]{:S(2)}) async-start(), calls=%async_computation.7 | async-start | bytes 2621440 | tf_op jit(solution)/shard_map/all_gather | solution.py:209
  10.5 63.4 %copy-start.11 = (f32[2048]{0:T(1024)S(1)}, f32[2048]{0:T(1024)}, u32[]{:S(2)}) copy-start(f32[2048]{0:T(1024)} %param.18) | copy-start | bytes 24580
  10.5 229.6 %all-gather.21.cloned.1.call-start = ((), (), s32[]{:S(2)}) async-start(), calls=%async_computation.6 | async-start | bytes 1966080 | tf_op jit(solution)/shard_map/all_gather | solution.py:214
  71.9 1.9 copy-start.2
  74.3 72.6 %copy-start = (bf16[384,2048]{1,0:T(8,128)(2,1)}, bf16[384,2048]{1,0:T(8,128)(2,1)S(1)}, u32[]{:S(2)}) copy-start(bf16[384,2048]{1,0:T(8,128)(2,1)S(1)} %fusion.27) | copy-start | bytes 4718596
  143.7 2.1 copy-start.3
  145.7 1.2 copy-start.4
  185.5 2.6 copy-start.5
  188.4 1.1 copy-start.10
  188.4 1.2 copy-start.12
  188.6 7.3 %copy-start.14 = (f32[64]{0:T(128)S(1)}, f32[64]{0:T(128)}, u32[]{:S(2)}) copy-start(f32[64]{0:T(128)} %get-tuple-element.195) | copy-start | bytes 772
  189.8 7.2 %collective-permute-start.1 = (bf16[128,2,64]{0,2,1:T(8,128)(2,1)S(1)}, bf16[128,2,64]{0,2,1:T(8,128)(2,1)S(1)}, u32[]{:S(2)}, u32[]{:S(2)}) collective-permute-start(bf16[128,2,64]{0,2,1:T(8,128)(2,1)S(1)} %slice.68), channel_id=1, source_target_pairs={{0,4},{4,8},{8,12},{1,5},{5,9},{9,13},{2,6},{6,10},{10,14},{3,7},{... | collective-permute-start | bytes 98312 | tf_op jit(solution)/shard_map/ppermute | solution.py:16
  192.6 5.4 %collective-permute-start = (bf16[128,2,64]{0,2,1:T(8,128)(2,1)S(1)}, bf16[128,2,64]{0,2,1:T(8,128)(2,1)S(1)}, u32[]{:S(2)}, u32[]{:S(2)}) collective-permute-start(bf16[128,2,64]{0,2,1:T(8,128)(2,1)S(1)} %bitcast.167), channel_id=1, source_target_pairs={{0,4},{4,8},{8,12},{1,5},{5,9},{9,13},{2,6},{6,10},{10,14},{3,7},{... | collective-permute-start | bytes 98312 | tf_op jit(solution)/shard_map/ppermute | solution.py:16
  197.3 1.2 copy-start.7
  198.5 0.7 copy-start.13
  200.9 1.5 copy-start.6
  202.4 120.1 %all-gather.11.cloned.1.call-start = ((), (), s32[]{:S(2)}) async-start(), calls=%async_computation.1 | async-start | bytes 5242880 | tf_op jit(solution)/shard_map/all_gather | solution.py:180
  203.8 118.7 %copy-start.1 = (bf16[384,2048]{1,0:T(8,128)(2,1)S(1)}, bf16[384,2048]{1,0:T(8,128)(2,1)}, u32[]{:S(2)}) copy-start(bf16[384,2048]{1,0:T(8,128)(2,1)} %copy-done) | copy-start | bytes 4718596
Sparse Core Ops, SparseCore 0:
  8.9 22.3 all-gather.8
  32.9 36.9 all-gather.14
  71.5 36.1 all-gather.16
  109.1 34.4 all-gather.18
  145.1 27.0 all-gather.12
  173.6 45.0 all-gather.22
  220.2 19.9 all-gather.20
  241.7 80.7 all-gather.10
where the time goes:
time: 341 us; the launch traced here: 340 us
  waiting for transfers between devices  134 us (39%)
  blocking collectives  107 us (31%)
  matrix products  37.9 us (11%)
  other arithmetic  23.1 us (7%)
  local copies, waits for them, and re-layouts  16.3 us (5%)
  between operations  14.7 us (4%)
  starting transfers between devices  6.38 us (2%)
    all_gather x1, waiting for transfers between devices, on_device(): lax.all_gather(merge_flat, 'sp', axis=0, tiled=True)  79.3 us
    all_gather x1, blocking collectives, forget_groups(): key_rows = lax.all_gather(keys, 'sp', axis=0, tiled=True)  25.4 us
    all_gather x1, blocking collectives, forget_groups(): value_rows = lax.all_gather(values, 'sp', axis=0, tiled=True)  25.2 us
    all_gather x1, waiting for transfers between devices, on_device(): lax.all_gather(head_stack, 'tp', axis=2, tiled=True)  21.5 us
    all_gather x1, blocking collectives, on_device(): lax.all_gather(w_value_window, 'sp', axis=0, tiled=True)  21.1 us
    all_gather x1, blocking collectives, on_device(): lax.all_gather(w_key_window, 'sp', axis=0, tiled=True)  19 us
    dot_general x7, matrix products, on_device(): jnp.dot(normed, weight_rows, preferred_element_type=jnp.float32)  16.8 us
    all_gather x1, blocking collectives, forget_groups(): gates_all = lax.all_gather(gates, 'sp', axis=0, tiled=True)  16.6 us
  transfers between devices with their start and end apart: 10, of which 6 were waited for; matrix products, arithmetic and copies ran while one was open for 20% of the time, Pallas kernels for 0%

commit v1 on v0

--- a/solution.py
+++ b/solution.py
@@ -112,8 +112,9 @@
         )
     )
     first_row = jnp.int32(0)
-    key_rows = lax.all_gather(keys, "sp", axis=0, tiled=True)
-    value_rows = lax.all_gather(values, "sp", axis=0, tiled=True)
+    right_arr = jnp.concatenate([keys, values], axis=1)
+    x_now = jax.lax.all_gather(right_arr, axis_name="sp", axis=0, tiled=True)
+    key_rows, value_rows = jnp.split(x_now, [keys.shape[1]], axis=1)
     piece_rows = key_rows.shape[0]
     sub_rows = math.gcd(piece_rows, 2048)
     turns = piece_rows // sub_rows

time: 341 us -> 357 us (1.047)
  waiting for transfers between devices: 134 us -> 197 us
  blocking collectives: 107 us -> 53 us
  local copies, waits for them, and re-layouts: 16.3 us -> 22 us
    all_gather x2 -> x0, blocking collectives: 50.7 us -> none  [the longest x1 25.4 us: forget_groups(): key_rows = lax.all_gather(keys, 'sp', axis=0, tiled=True)]
    all_gather x1, waiting for transfers between devices: 79.3 us -> 44.1 us  [on_device(): lax.all_gather(merge_flat, 'sp', axis=0, tiled=True)]
    all_gather x1, waiting for transfers between devices: 0.02 us -> 27.2 us  [on_device(): lax.all_gather(w_key_forget, 'sp', axis=0, tiled=True)]
    all_gather x1, waiting for transfers between devices: 14.9 us -> 36.6 us  [on_device(): branch_full = lax.all_gather(w_branch, 'sp', axis=1, tiled=True)]
    all_gather x1, waiting for transfers between devices: 5.25 us -> 26.8 us  [on_device(): lax.all_gather(w_value_forget, 'sp', axis=0, tiled=True)]
    all_gather x1, waiting for transfers between devices: 0.01 us -> 19.9 us  [on_device(): gathered = lax.all_gather(tokens, 'tp', axis=1, tiled=True)]
    all_gather x0 -> x1, waiting for transfers between devices: none -> 15.1 us  [forget_groups(): x_now = jax.lax.all_gather(right_arr, axis_name='sp', axis=0, tiled=True)]
    all_gather x1, waiting for transfers between devices: 8.71 us -> 0.01 us  [on_device(): lax.all_gather(w_query_forget, 'sp', axis=0, tiled=True)]
  transfers between devices with their start and end apart: 10 -> 11, of which waited for: 6 -> 8; matrix products, arithmetic and copies ran while one was open for 20% -> 22% of each run, Pallas kernels for 0% -> 0%
where the time goes in v1:
time: 357 us; the launch traced here: 356 us
  waiting for transfers between devices  197 us (55%)
  blocking collectives  53 us (15%)
  matrix products  37 us (10%)
  other arithmetic  24.8 us (7%)
  local copies, waits for them, and re-layouts  22 us (6%)
  between operations  14.3 us (4%)
  starting transfers between devices  7.03 us (2%)
    all_gather x1, waiting for transfers between devices, on_device(): lax.all_gather(merge_flat, 'sp', axis=0, tiled=True)  44.1 us
    all_gather x1, waiting for transfers between devices, on_device(): branch_full = lax.all_gather(w_branch, 'sp', axis=1, tiled=True)  36.6 us
    all_gather x1, waiting for transfers between devices, on_device(): lax.all_gather(w_key_forget, 'sp', axis=0, tiled=True)  27.2 us
    all_gather x1, waiting for transfers between devices, on_device(): lax.all_gather(w_value_forget, 'sp', axis=0, tiled=True)  26.8 us
    all_gather x1, waiting for transfers between devices, on_device(): lax.all_gather(head_stack, 'tp', axis=2, tiled=True)  20.2 us
    all_gather x1, blocking collectives, on_device(): lax.all_gather(w_value_window, 'sp', axis=0, tiled=True)  20 us
    all_gather x1, waiting for transfers between devices, on_device(): gathered = lax.all_gather(tokens, 'tp', axis=1, tiled=True)  19.9 us
    all_gather x1, blocking collectives, on_device(): lax.all_gather(w_key_window, 'sp', axis=0, tiled=True)  18.5 us
  transfers between devices with their start and end apart: 11, of which 8 were waited for; matrix products, arithmetic and copies ran while one was open for 22% of the time, Pallas kernels for 0%

profile of v1, /device:TPU:0, one launch (start us, length us, event | category | flops | bytes accessed | tf_op | source)
XLA Modules:
  0.0 355.5 jit_solution(10191989620739413122)
XLA Ops:
  6.5 0.7 all-gather.10.cloned.1.call-update
  10.0 1.4 slice_bitcast_fusion.2
  11.4 19.9 %all-gather.10.cloned.1.call-done = bf16[384,2048]{1,0:T(8,128)(2,1)} async-done(((bf16[384,512]{1,0:T(8,128)(2,1)}), bf16[384,2048]{1,0:T(8,128)(2,1)}) %all-gather.10.cloned.1.call-update) | async-done | bytes 1572880 | tf_op jit(solution)/shard_map/all_gather | solution.py:166
  31.3 1.9 fusion.25
  33.7 27.2 %all-gather.16.cloned.1.call-done = bf16[2048,256]{1,0:T(8,128)(2,1)} async-done(((bf16[512,256]{1,0:T(8,128)(2,1)}), bf16[2048,256]{1,0:T(8,128)(2,1)}) %all-gather.16.cloned.1.call-update) | async-done | bytes 1048592 | tf_op jit(solution)/shard_map/all_gather | solution.py:179
  60.9 2.0 multiply_reduce_fusion.1
  63.0 26.8 %all-gather.18.cloned.1.call-done = bf16[2048,256]{1,0:T(8,128)(2,1)} async-done(((bf16[512,256]{1,0:T(8,128)(2,1)}), bf16[2048,256]{1,0:T(8,128)(2,1)}) %all-gather.18.cloned.1.call-update) | async-done | bytes 1048592 | tf_op jit(solution)/shard_map/all_gather | solution.py:180
  89.8 2.0 convolution_convert_fusion.1
  91.8 0.8 pad_maximum_fusion
  92.7 1.3 copy.55
  95.4 1.2 slice.58
  97.3 14.4 %all_gather.44 = f32[1536,4]{0,1:T(4,128)} all-gather(f32[384,4]{0,1:T(4,128)} %param.27), channel_id=1, replica_groups=mesh['grp'=2,'sp'=4,'tp'=4] {'sp'}, dimensions={0}, use_global_device_ids=true | all-gather | bytes 30720 | tf_op jit(solution)/shard_map/all_gather | solution.py:76
  111.8 18.5 %all_gather.39 = bf16[2048,128]{1,0:T(8,128)(2,1)S(1)} all-gather(bf16[512,128]{1,0:T(8,128)(2,1)S(1)} %copy-done.9), channel_id=1, replica_groups=mesh['grp'=2,'sp'=4,'tp'=4] {'sp'}, dimensions={0}, use_global_device_ids=true | all-gather | bytes 655360 | tf_op jit(solution)/shard_map/all_gather | solution.py:176
  130.5 20.0 %all_gather.38 = bf16[2048,128]{1,0:T(8,128)(2,1)S(1)} all-gather(bf16[512,128]{1,0:T(8,128)(2,1)S(1)} %copy-done.10), channel_id=1, replica_groups=mesh['grp'=2,'sp'=4,'tp'=4] {'sp'}, dimensions={0}, use_global_device_ids=true | all-gather | bytes 655360 | tf_op jit(solution)/shard_map/all_gather | solution.py:177
  151.2 2.8 multiply_reduce_fusion
  154.0 3.6 %all-gather.14.cloned.1.call-done = bf16[2048,256]{1,0:T(8,128)(2,1)} async-done(((bf16[512,256]{1,0:T(8,128)(2,1)}), bf16[2048,256]{1,0:T(8,128)(2,1)}) %all-gather.14.cloned.1.call-update) | async-done | bytes 1048592 | tf_op jit(solution)/shard_map/all_gather | solution.py:175
  157.6 2.0 bitcast_reduce_fusion
  159.6 0.9 copy.38
  160.5 1.5 reshape.266
  162.1 1.0 copy.39
  163.1 1.2 multiply_reduce_fusion.2
  164.3 1.0 reshape.274
  165.5 1.0 multiply_convert_fusion.3
  167.1 3.5 collective-permute-start.1
  171.3 3.2 collective-permute-start
  174.6 1.0 multiply_convert_fusion
  175.7 0.8 multiply_convert_fusion.1
  179.2 1.0 fusion.32
  180.8 15.1 %all-gather.20.cloned.1.call-done = bf16[1536,8,64]{0,2,1:T(8,128)(2,1)} async-done(((bf16[384,8,64]{0,2,1:T(8,128)(2,1)}), bf16[1536,8,64]{0,2,1:T(8,128)(2,1)}) %all-gather.20.cloned.1.call-update) | async-done | bytes 1572880 | tf_op jit(solution)/shard_map/all_gather | solution.py:116
  195.9 36.8 %conditional.1 = (f32[4,384]{1,0:T(4,128)}, f32[384,4,64]{0,2,1:T(8,128)}) conditional(s32[]{:T(128)} %bitcast.13, () %tuple.20, (bf16[1536,8,64]{0,2,1:T(8,128)(2,1)}, f32[1536,4]{0,1:T(4,128)}, s32[3,512]{1,0:T(4,128)S(1)}, s32[3,512]{1,0:T(4,128)S(1)}, s32[384]{0:T(512)}, /*index=5*/bf16[384,4,64]{0,2,1:T(8,128)(2,1)}, f32[384,4]{0,1:T(4,128)}) %tuple.21), branch_computations={%region_7.8_spmd, %region_8.13_spmd} | conditional | flops 215199744 | bytes 18206496 | solution.py:139
  196.6 1.5 fusion.56
  198.0 1.3 copy_bitcast_fusion
  199.3 33.4 %while.18 = (s32[]{:T(128)}, f32[4,384]{1,0:T(4,128)S(1)}, f32[4,384]{1,0:T(4,128)}, f32[384,4,64]{0,2,1:T(8,128)}, s32[384]{0:T(512)}, /*index=5*/s32[3,512]{1,...) while((s32[]{:T(128)}, f32[4,384]{1,0:T(4,128)S(1)}, ...), condition=%wide.region_12.12_spmd.clone, body=%wide.region_9.11_spmd.clone.sunk | while | flops 215196672 | bytes 11896481 | solution.py:134
  200.0 0.7 constant_dynamic-slice_fusion.2
  200.7 0.8 broadcast_compare_fusion.2
  201.6 2.7 fusion.86
  204.2 0.7 fusion.87
  204.9 1.6 fusion.88
  207.2 2.8 fusion.90
  210.6 0.7 constant_dynamic-slice_fusion.2
  211.3 0.8 broadcast_compare_fusion.2
  212.2 2.7 fusion.86
  214.8 0.7 fusion.87
  215.5 1.6 fusion.88
  217.2 1.3 fusion.89
  218.5 2.9 fusion.90
  221.3 0.7 dynamic-slice_bitcast_fusion.2
  222.0 0.7 constant_dynamic-slice_fusion.2
  222.7 0.8 broadcast_compare_fusion.2
  223.5 2.7 fusion.86
  226.2 0.7 fusion.87
  226.9 1.6 fusion.88
  228.6 1.3 fusion.89
  229.9 2.9 fusion.90
  232.7 1.1 divide_convert_fusion.2
  234.1 0.8 pad_maximum_fusion.1
  234.9 44.1 %all-gather.12.cloned.1.call-done = bf16[2048,1024]{1,0:T(8,128)(2,1)} async-done(((bf16[512,1024]{1,0:T(8,128)(2,1)}), bf16[2048,1024]{1,0:T(8,128)(2,1)}) %all-gather.12.cloned.1.call-update) | async-done | bytes 4194320 | tf_op jit(solution)/shard_map/all_gather | solution.py:181
  279.0 5.3 %add_divide_fusion = f32[384,1024]{1,0:T(8,128)} fusion(bf16[384,2048]{1,0:T(8,128)(2,1)S(1)} %copy-done.1, bf16[2048,1024]{1,0:T(8,128)(2,1)} %all-gather.12.cloned.1.call-done), kind=kOutput, calls=%fused_computation.44 | convolution fusion | flops 1611792384 | bytes 7340032 | tf_op jit(solution)/shard_map/dot_general | solution.py:184
  284.2 2.7 reshape.258
  286.9 1.2 fusion.57
  288.1 36.6 %all-gather.26.cloned.1.call-done = bf16[2,1024,512]{2,1,0:T(8,128)(2,1)} async-done(((bf16[2,256,512]{2,1,0:T(8,128)(2,1)}), bf16[2,1024,512]{2,1,0:T(8,128)(2,1)}) %all-gather.26.cloned.1.call-update) | async-done | bytes 2097168 | tf_op jit(solution)/shard_map/all_gather | solution.py:210
  324.7 20.2 %all-gather.24.cloned.1.call-done = bf16[384,2,1024]{2,0,1:T(8,128)(2,1)} async-done(((bf16[384,2,256]{2,0,1:T(8,128)(2,1)}), bf16[384,2,1024]{2,0,1:T(8,128)(2,1)}) %all-gather.24.cloned.1.call-update) | async-done | bytes 1572880 | tf_op jit(solution)/shard_map/all_gather | solution.py:215
  344.9 3.0 convolution_bitcast_fusion
  348.0 1.0 fusion.36
  (102 shorter events, 13.1 us)
Async XLA Ops:
  6.5 26.7 %copy-start.11 = (f32[2048]{0:T(1024)S(1)}, f32[2048]{0:T(1024)}, u32[]{:S(2)}) copy-start(f32[2048]{0:T(1024)} %param.18) | copy-start | bytes 24580
  6.5 24.7 %all-gather.10.cloned.1.call-start = ((), (), s32[]{:S(2)}) async-start(), calls=%async_computation | async-start | bytes 1966080 | tf_op jit(solution)/shard_map/all_gather | solution.py:166
  7.3 53.6 %all-gather.16.cloned.1.call-start = ((), (), s32[]{:S(2)}) async-start(), calls=%async_computation.3 | async-start | bytes 1310720 | tf_op jit(solution)/shard_map/all_gather | solution.py:179
  8.0 81.8 %all-gather.18.cloned.1.call-start = ((), (), s32[]{:S(2)}) async-start(), calls=%async_computation.4 | async-start | bytes 1310720 | tf_op jit(solution)/shard_map/all_gather | solution.py:180
  8.7 142.4 %all-gather.22.cloned.1.call-start = ((), (), s32[]{:S(2)}) async-start(), calls=%async_computation.6 | async-start | bytes 1310720 | tf_op jit(solution)/shard_map/all_gather | solution.py:178
  9.3 148.3 %all-gather.14.cloned.1.call-start = ((), (), s32[]{:S(2)}) async-start(), calls=%async_computation.2 | async-start | bytes 1310720 | tf_op jit(solution)/shard_map/all_gather | solution.py:175
  9.9 186.0 %all-gather.20.cloned.1.call-start = ((), (), s32[]{:S(2)}) async-start(), calls=%async_computation.5 | async-start | bytes 1966080 | tf_op jit(solution)/shard_map/all_gather | solution.py:116
  31.3 1.9 copy-start.2
  33.7 137.0 %copy-start = (bf16[384,2048]{1,0:T(8,128)(2,1)}, bf16[384,2048]{1,0:T(8,128)(2,1)S(1)}, u32[]{:S(2)}) copy-start(bf16[384,2048]{1,0:T(8,128)(2,1)S(1)} %fusion.27) | copy-start | bytes 4718596
  63.0 29.7 %copy-start.5 = (bf16[512,2,512]{2,1,0:T(2,128)(2,1)S(1)}, bf16[512,2,512]{2,1,0:T(2,128)(2,1)}, u32[]{:S(2)}) copy-start(bf16[512,2,512]{2,1,0:T(2,128)(2,1)} %param.28) | copy-start | bytes 3145732
  92.6 186.3 %all-gather.12.cloned.1.call-start = ((), (), s32[]{:S(2)}) async-start(), calls=%async_computation.1 | async-start | bytes 5242880 | tf_op jit(solution)/shard_map/all_gather | solution.py:181
  92.7 19.1 %copy-start.9 = (bf16[512,128]{1,0:T(8,128)(2,1)S(1)}, bf16[512,128]{1,0:T(8,128)(2,1)}, u32[]{:S(2)}) copy-start(bf16[512,128]{1,0:T(8,128)(2,1)} %param.21) | copy-start | bytes 393220
  94.0 36.4 %copy-start.14 = (f32[4]{0:T(128)S(1)}, f32[4]{0:T(128)}, u32[]{:S(2)}) copy-start(f32[4]{0:T(128)} %param.23) | copy-start | bytes 52
  94.0 36.5 %copy-start.10 = (bf16[512,128]{1,0:T(8,128)(2,1)S(1)}, bf16[512,128]{1,0:T(8,128)(2,1)}, u32[]{:S(2)}) copy-start(bf16[512,128]{1,0:T(8,128)(2,1)} %param.22) | copy-start | bytes 393220
  94.0 230.7 %all-gather.26.cloned.1.call-start = ((), (), s32[]{:S(2)}) async-start(), calls=%async_computation.8 | async-start | bytes 2621440 | tf_op jit(solution)/shard_map/all_gather | solution.py:210
  94.8 250.2 %all-gather.24.cloned.1.call-start = ((), (), s32[]{:S(2)}) async-start(), calls=%async_computation.7 | async-start | bytes 1966080 | tf_op jit(solution)/shard_map/all_gather | solution.py:215
  166.5 0.6 copy-start.6
  166.5 8.1 %copy-start.4 = (f32[6,64,2,2]{3,2,1,0:T(2,128)S(1)}, f32[6,64,2,2]{3,2,1,0:T(2,128)}, u32[]{:S(2)}) copy-start(f32[6,64,2,2]{3,2,1,0:T(2,128)} %copy.39) | copy-start | bytes 18436
  166.5 8.1 %copy-start.12 = (f32[64]{0:T(128)S(1)}, f32[64]{0:T(128)}, u32[]{:S(2)}) copy-start(f32[64]{0:T(128)} %get-tuple-element.197) | copy-start | bytes 772
  167.1 9.5 %collective-permute-start.1 = (bf16[128,2,64]{0,2,1:T(8,128)(2,1)}, bf16[128,2,64]{0,2,1:T(8,128)(2,1)S(1)}, u32[]{:S(2)}, u32[]{:S(2)}) collective-permute-start(bf16[128,2,64]{0,2,1:T(8,128)(2,1)} %slice.68), channel_id=1, source_target_pairs={{0,4},{4,8},{8,12},{1,5},{5,9},{9,13},{2,6},{6,10},{10,14},{3,7},{... | collective-permute-start | bytes 98312 | tf_op jit(solution)/shard_map/ppermute | solution.py:16
  171.3 4.4 %copy-start.3 = (f32[384,256]{0,1:T(8,128)S(1)}, f32[384,256]{0,1:T(8,128)}, u32[]{:S(2)}) copy-start(f32[384,256]{0,1:T(8,128)} %get-tuple-element.204) | copy-start | bytes 1179652
  171.3 4.4 %copy-start.13 = (f32[64]{0:T(128)S(1)}, f32[64]{0:T(128)}, u32[]{:S(2)}) copy-start(f32[64]{0:T(128)} %get-tuple-element.199) | copy-start | bytes 772
  171.3 5.9 %collective-permute-start = (bf16[128,2,64]{0,2,1:T(8,128)(2,1)S(1)}, bf16[128,2,64]{0,2,1:T(8,128)(2,1)S(1)}, u32[]{:S(2)}, u32[]{:S(2)}) collective-permute-start(bf16[128,2,64]{0,2,1:T(8,128)(2,1)S(1)} %bitcast.167), channel_id=1, source_target_pairs={{0,4},{4,8},{8,12},{1,5},{5,9},{9,13},{2,6},{6,10},{10,14},{3,7},{... | collective-permute-start | bytes 98312 | tf_op jit(solution)/shard_map/ppermute | solution.py:16
  174.6 2.1 copy-start.7
  177.0 0.9 copy-start.8
  232.7 46.2 %copy-start.1 = (bf16[384,2048]{1,0:T(8,128)(2,1)S(1)}, bf16[384,2048]{1,0:T(8,128)(2,1)}, u32[]{:S(2)}) copy-start(bf16[384,2048]{1,0:T(8,128)(2,1)} %copy-done) | copy-start | bytes 4718596
Sparse Core Ops, SparseCore 0:
  8.9 22.3 all-gather.9
  32.8 27.9 all-gather.15
  62.4 27.3 all-gather.17
  91.3 33.3 all-gather.21
  126.1 31.5 all-gather.13
  159.0 36.8 all-gather.19
  197.5 81.4 all-gather.11
  280.5 44.1 all-gather.25
  326.3 18.6 all-gather.23
